TPU v7x, 32 devices: a whole 2x2x4 slice. The times are simulated.
32 devices in a mesh: fs: 8 (over z, y), tp: 4 (over x, core).
Axes of the slice: x: 2, y: 2, z: 4, core: 2. Of those that a mesh axis runs over, the one named last changes fastest.
Arguments:
- tokens: bfloat16 [12288, 2048], P('fs', 'tp'), may hold values from -6 to 6
- norm_gain: float32 [2048], P('fs'), may hold values from 0.1 to 1.9
- up_weight: float32 [2048, 8192], P('fs', 'tp'), may hold values from -0.125 to 0.125
- down_weight: float32 [2048, 8192], P('fs', 'tp'), may hold values from -0.0625 to 0.0625
Outputs:
- up_matrix: bfloat16 [2048, 8192], P(None, 'tp')
- down_matrix: bfloat16 [2048, 8192], P(None, 'tp')
- mixed: bfloat16 [12288, 2048], P('fs', 'tp')
All inputs are finite; a program needn't handle non-finite values.
Results may differ from a plain program's by a relative error of at most 0.0095.
Values may be sent and summed in bfloat16 or wider, within the bound.
A program may use at most 128 MiB of HBM per device.

v0:
```python
import jax
import jax.numpy as jnp
from jax import lax
from jax.sharding import PartitionSpec as P

epsilon = 1e-06


def row_scale(full_rows):
    widened = full_rows.astype(jnp.float32)
    scaled = widened * lax.rsqrt(jnp.mean(widened * widened, axis=-1, keepdims=True) + epsilon)
    return scaled.astype(jnp.bfloat16)


def on_device(tokens, norm_gain, up_weight, down_weight):
    up_local = (norm_gain[:, None] * up_weight).astype(jnp.bfloat16)
    down_local = down_weight.astype(jnp.bfloat16)
    full_rows = lax.all_gather(tokens, "tp", axis=1, tiled=True)
    normed = row_scale(full_rows)
    up_matrix = lax.all_gather(up_local, "fs", axis=0, tiled=True)
    up_values = jnp.dot(normed, up_matrix, preferred_element_type=jnp.float32)
    hidden = jnp.square(jax.nn.relu(up_values)).astype(jnp.bfloat16)
    block_rows = lax.all_gather(down_local, "fs", axis=0, tiled=True)
    products = lax.dot_general(
        hidden, block_rows, (((1,), (1,)), ((), ())), preferred_element_type=jnp.float32
    )
    rounded = products.astype(jnp.bfloat16).astype(jnp.float32)
    mixed = lax.psum_scatter(rounded.astype(jnp.bfloat16), "tp", scatter_dimension=1, tiled=True)
    return (up_matrix, block_rows, mixed)


def solution(mesh):
    return jax.shard_map(
        on_device,
        mesh=mesh,
        in_specs=(P("fs", "tp"), P("fs"), P("fs", "tp"), P("fs", "tp")),
        out_specs=(P(None, "tp"), P(None, "tp"), P("fs", "tp")),
        check_vma=False,
    )
```

profile of v0, /device:TPU:7, one launch (start us, length us, event | category | flops | bytes accessed | tf_op | source)
XLA Modules:
  0.0 422.9 jit_solution(17466256598558638301)
XLA Ops:
  7.2 0.0 all-gather.8.cloned.1.call-start
  7.2 0.7 all-gather.8.cloned.1.call-update
  7.9 0.0 all-gather.4.cloned.1.call-start
  7.9 2.7 multiply_convert_fusion.1
  10.7 0.0 all-gather.4.cloned.1.call-update
  10.7 0.0 all-gather.6.cloned.1.call-start
  10.8 2.7 convert_element_type.21
  13.5 0.0 all-gather.6.cloned.1.call-update
  13.5 0.0 reduce-scatter.2.cloned.1.call-start
  13.6 43.1 %all-gather.8.cloned.1.call-done = bf16[1536,2048]{1,0:T(8,128)(2,1)} async-done(((bf16[1536,512]{1,0:T(8,128)(2,1)}), bf16[1536,2048]{1,0:T(8,128)(2,1)}) %all-gather.8.cloned.1.call-update) | async-done | bytes 6291472 | tf_op jit(solution)/shard_map/all_gather | solution.py:18
  56.6 4.1 fusion
  60.7 122.0 %all-gather.4.cloned.1.call-done = bf16[2048,2048]{1,0:T(8,128)(2,1)} async-done(((bf16[256,2048]{1,0:T(8,128)(2,1)}), bf16[2048,2048]{1,0:T(8,128)(2,1)}) %all-gather.4.cloned.1.call-update) | async-done | bytes 8388624 | tf_op jit(solution)/shard_map/all_gather | solution.py:20
  182.7 125.4 %all-gather.6.cloned.1.call-done = bf16[2048,2048]{1,0:T(8,128)(2,1)} async-done(((bf16[256,2048]{1,0:T(8,128)(2,1)}), bf16[2048,2048]{1,0:T(8,128)(2,1)}) %all-gather.6.cloned.1.call-update) | async-done | bytes 8388624 | tf_op jit(solution)/shard_map/all_gather | solution.py:23
  308.1 34.7 %fusion.3 = bf16[1536,2048]{1,0:T(8,128)(2,1)} fusion(bf16[2048,2048]{1,0:T(8,128)(2,1)} %all-gather.6.cloned.1.call-done, bf16[2048,2048]{1,0:T(8,128)(2,1)} %all-gather.4.cloned.1.call-done, bf16[1536,2048]{1,0:T(8,128)(2,1)} %all-gather.8.cloned.1.call-done, f32[1536]{0:T(1024)S(1)} %add_rsqrt_fusion), kind=kOutput, calls=%fused_computation.6 | convolution fusion | flops 25791823872 | bytes 29366272 | tf_op jit(solution)/shard_map/dot_general | solution.py:24
  342.7 0.0 reduce-scatter.2.cloned.1.call-update
  342.7 56.8 %reduce-scatter.2.cloned.1.call-done = bf16[1536,512]{1,0:T(8,128)(2,1)} async-done(((bf16[1536,2048]{1,0:T(8,128)(2,1)}), bf16[1536,512]{1,0:T(8,128)(2,1)}) %reduce-scatter.2.cloned.1.call-update) | async-done | bytes 1572880 | tf_op jit(solution)/shard_map/reduce_scatter | solution.py:28
  399.5 8.4 %copy.9 = bf16[2048,2048]{1,0:T(8,128)(2,1)} copy(bf16[2048,2048]{1,0:T(8,128)(2,1)} %all-gather.4.cloned.1.call-done) | data formatting | bytes 16777216
  408.0 8.4 %copy.10 = bf16[2048,2048]{1,0:T(8,128)(2,1)} copy(bf16[2048,2048]{1,0:T(8,128)(2,1)} %all-gather.6.cloned.1.call-done) | data formatting | bytes 16777216
  (1 shorter events, 0.0 us)
Async XLA Ops:
  7.2 49.4 %all-gather.8.cloned.1.call-start = ((), (), s32[]{:S(2)}) async-start(), calls=%async_computation.3 | async-start | bytes 7864320 | tf_op jit(solution)/shard_map/all_gather | solution.py:18
  7.9 174.8 %all-gather.4.cloned.1.call-start = ((), (), s32[]{:S(2)}) async-start(), calls=%async_computation.1 | async-start | bytes 9437184 | tf_op jit(solution)/shard_map/all_gather | solution.py:20
  10.7 297.4 %all-gather.6.cloned.1.call-start = ((), (), s32[]{:S(2)}) async-start(), calls=%async_computation.2 | async-start | bytes 9437184 | tf_op jit(solution)/shard_map/all_gather | solution.py:23
  13.5 386.0 %reduce-scatter.2.cloned.1.call-start = ((), (), s32[]{:S(2)}) async-start(), calls=%async_computation.4 | async-start | bytes 7864320 | tf_op jit(solution)/shard_map/reduce_scatter | solution.py:28
Sparse Core Ops, SparseCore 0:
  9.5 47.0 all-gather.7
  59.3 123.3 all-gather.3
  185.4 122.6 all-gather.5
  342.9 56.6 reduce-scatter.1
where the time goes:
time: 426 us; the launch traced here: 423 us
  waiting for transfers between devices  348 us (82%)
  matrix products  34.7 us (8%)
  local copies, waits for them, and re-layouts  16.9 us (4%)
  between operations  13.8 us (3%)
  other arithmetic  9.54 us (2%)
    all_gather x1, waiting for transfers between devices, on_device(): block_rows = lax.all_gather(down_local, 'fs', axis=0, tiled=True)  125 us
    all_gather x1, waiting for transfers between devices, on_device(): up_matrix = lax.all_gather(up_local, 'fs', axis=0, tiled=True)  122 us
    reduce_scatter x1, waiting for transfers between devices, on_device(): lax.psum_scatter(rounded.astype(jnp.bfloat16), 'tp', scatter_dimension=1,...  56.8 us
    all_gather x1, waiting for transfers between devices, on_device(): full_rows = lax.all_gather(tokens, 'tp', axis=1, tiled=True)  43.1 us
    dot_general x1, matrix products, on_device(): lax.dot_general(hidden, block_rows, (((1,), (1,)), ((), ())), preferred_e...  34.7 us
    unnamed x2, local copies, waits for them, and re-layouts  16.9 us
  transfers between devices with their start and end apart: 4, of which 4 were waited for; matrix products, arithmetic and copies ran while one was open for 2% of the time, Pallas kernels for 0%

commit v1 on v0

v1 whole, which is shorter than its diff:
```python
import functools

import jax
import jax.numpy as jnp
from jax import lax
from jax.experimental import pallas as pl
from jax.experimental.pallas import tpu as pltpu
from jax.sharding import PartitionSpec as P

epsilon = 1e-06
MESH = pl.DeviceIdType.MESH
UP, DOWN, SIDE = 0, 1, 2


def chunks_of(rows):
    extra = max(16, rows // 8 // 16 * 16)
    main = rows - extra
    if main % 32 == 0:
        half = main // 2
        return [(0, half), (half, half), (main, extra)]
    return [(0, main), (main, extra)]


def kernel(n, tp, tok_in, upl, downl, up_out, down_out, mixed_out,
           tok, up, down, hidden, part, pair, cross, total,
           send_sem, recv_sem, tok_send, tok_recv, pair_send, pair_recv, cross_send, cross_recv, local_sem):
    rows = upl.shape[0]
    tokens, width = tok_in.shape
    chain = n // 2
    groups = tp // 2
    per_owner = n // tp
    chunks = chunks_of(rows)
    extra = len(chunks) - 1
    mains = range(extra)
    fs, me = lax.axis_index("fs"), lax.axis_index("tp")
    z, y = fs // 2, fs % 2
    group, core = me // 2, me % 2
    partner = group * 2 + 1 - core
    bufs = (up, down)
    mine = (upl, downl)

    def target(way):
        if way == UP:
            return {"fs": jnp.minimum(z + 1, chain - 1) * 2 + y}
        if way == DOWN:
            return {"fs": jnp.maximum(z - 1, 0) * 2 + y}
        return {"fs": z * 2 + 1 - y}

    def spot(src, k):
        return pl.ds(pl.multiple_of(src * rows, 16) + chunks[k][0], chunks[k][1])

    def copy(m, src, k, way, own):
        where = spot(src, k)
        return pltpu.make_async_remote_copy(
            src_ref=mine[m].at[pl.ds(*chunks[k])] if own else bufs[m].at[where],
            dst_ref=bufs[m].at[where],
            send_sem=send_sem.at[m, way, src, k],
            recv_sem=recv_sem.at[m, src, k],
            device_id=target(way),
            device_id_type=MESH,
        )

    def arrived(m, src, k):
        where = spot(src, k)
        pltpu.make_async_remote_copy(
            src_ref=bufs[m].at[where], dst_ref=bufs[m].at[where],
            send_sem=send_sem.at[m, SIDE, src, k], recv_sem=recv_sem.at[m, src, k],
            device_id=target(SIDE), device_id_type=MESH,
        ).wait_recv()

    def own_sends(m):
        order = [(SIDE, extra)] + [(way, k) for k in mains for way in (UP, DOWN, SIDE)] + [(UP, extra), (DOWN, extra)]
        return [(way, k) for way, k in order]

    def when_way(way, fn):
        if way == UP:
            pl.when(z < chain - 1)(fn)
        elif way == DOWN:
            pl.when(z > 0)(fn)
        else:
            fn()

    def start_own(m):
        for way, k in own_sends(m):
            when_way(way, lambda way=way, k=k: copy(m, fs, k, way, True).start())

    def relay_own_extra(m, act):
        other = z * 2 + 1 - y
        for way in (UP, DOWN):
            when_way(way, lambda way=way: act(copy(m, other, extra, way, False)))

    def step_sends(m, d, act, wait):
        plan = [(k, 0) for k in mains] + [(extra, 0), (extra, 1)]
        for k, flip in plan:
            for sign, way in ((-1, UP), (1, DOWN)):
                at = z + sign * d
                src = at * 2 + (y + flip) % 2

                @pl.when((at >= 0) & (at < chain))
                def _():
                    if wait:
                        arrived(m, src, k)
                    when_way(way, lambda: act(copy(m, src, k, way, False)))
                    if k != extra:
                        act(copy(m, src, k, SIDE, False))

    def side_arrivals(m, d):
        for sign in (-1, 1) if not (isinstance(d, int) and d == 0) else (1,):
            at = z + sign * d

            @pl.when((at >= 0) & (at < chain))
            def _():
                for k in mains:
                    arrived(m, at * 2 + 1 - y, k)

    barrier = pltpu.get_barrier_semaphore()
    greet = [{"fs": lax.rem(z + 1, chain) * 2 + y}, {"fs": lax.rem(z + chain - 1, chain) * 2 + y},
             {"fs": z * 2 + 1 - y}, {"tp": partner}]
    greet += [{"tp": lax.rem(group + g, groups) * 2 + core} for g in range(1, groups)]
    for who in greet:
        pl.semaphore_signal(barrier, inc=1, device_id=who, device_id_type=MESH)
    pl.semaphore_wait(barrier, len(greet))

    start_own(0)

    def columns(owner):
        return pl.ds(pl.multiple_of(owner * width, 128), width)

    def token_copy(owner, to, slot, own):
        return pltpu.make_async_remote_copy(
            src_ref=tok_in if own else tok.at[:, columns(owner)],
            dst_ref=tok.at[:, columns(owner)],
            send_sem=tok_send.at[slot], recv_sem=tok_recv.at[owner],
            device_id={"tp": to}, device_id_type=MESH)

    across = [lax.rem(group + g, groups) * 2 + core for g in range(1, groups)]
    back = [lax.rem(group + groups - g, groups) * 2 + core for g in range(1, groups)]
    token_sends = [token_copy(me, to, i, True) for i, to in enumerate(across)]
    token_sends.append(token_copy(me, partner, groups - 1, True))
    for c in token_sends:
        c.start()
    own_tokens = pltpu.make_async_copy(tok_in, tok.at[:, columns(me)], local_sem.at[0])
    own_tokens.start()
    own_rows = pl.ds(pl.multiple_of(fs * rows, 16), rows)
    own_up = pltpu.make_async_copy(upl, up.at[own_rows], local_sem.at[1])
    own_up.start()
    own_down = pltpu.make_async_copy(downl, down.at[own_rows], local_sem.at[2])
    own_down.start()

    arrived(0, z * 2 + 1 - y, extra)
    relay_own_extra(0, lambda c: c.start())
    step_sends(0, 1, lambda c: c.start(), True)

    relays = []
    for i, owner in enumerate(back):
        token_copy(owner, partner, groups + i, False).wait_recv()
        c = token_copy(owner, partner, groups + i, False)
        c.start()
        relays.append(c)
    token_copy(partner, partner, 0, False).wait_recv()
    for g in range(1, groups):
        token_copy(lax.rem(group + g, groups) * 2 + 1 - core, partner, 0, False).wait_recv()
    for c in token_sends + relays:
        c.wait_send()
    own_tokens.wait()
    tile = 128

    @pl.loop(0, tokens // tile)
    def _(i):
        at = pl.ds(pl.multiple_of(i * tile, tile), tile)
        wide = tok[at, :].astype(jnp.float32)
        scale = lax.rsqrt(jnp.mean(wide * wide, axis=-1, keepdims=True) + epsilon)
        tok[at, :] = (wide * scale).astype(jnp.bfloat16)

    for d in range(2, chain):
        step_sends(0, d, lambda c: c.start(), True)
    start_own(1)
    for d in range(chain):
        side_arrivals(0, d)
    arrived(1, z * 2 + 1 - y, extra)
    relay_own_extra(1, lambda c: c.start())
    step_sends(1, 1, lambda c: c.start(), True)
    own_up.wait()
    up_write = pltpu.make_async_copy(up, up_out, local_sem.at[1])
    up_write.start()

    bm, bn = min(512, tokens), min(512, up.shape[1])

    @pl.loop(0, up.shape[1] // bn)
    def _(j):
        cols = pl.ds(pl.multiple_of(j * bn, bn), bn)

        @pl.loop(0, tokens // bm)
        def _(i):
            at = pl.ds(pl.multiple_of(i * bm, bm), bm)
            values = jnp.dot(tok[at, :], up[:, cols], preferred_element_type=jnp.float32)
            values = jnp.maximum(values, 0.0)
            hidden[at, cols] = (values * values).astype(jnp.bfloat16)

    def pair_copy(r):
        return pltpu.make_async_remote_copy(
            src_ref=part.at[r], dst_ref=pair.at[r], send_sem=pair_send.at[r], recv_sem=pair_recv.at[r],
            device_id={"tp": partner}, device_id_type=MESH)

    def cross_copy(r, to_group, from_group):
        return pltpu.make_async_remote_copy(
            src_ref=part.at[r], dst_ref=cross.at[from_group, r % per_owner],
            send_sem=cross_send.at[r], recv_sem=cross_recv.at[from_group, r % per_owner],
            device_id={"tp": to_group * 2 + core}, device_id_type=MESH)

    def block_write(r):
        where = pl.ds(pl.multiple_of(r * rows, 16), rows)
        return pltpu.make_async_copy(down.at[where], down_out.at[where], local_sem.at[3 + r])

    def multiply(r):
        block_write(r).start()
        where = pl.ds(pl.multiple_of(r * rows, 16), rows)

        @pl.loop(0, tokens // bm)
        def _(i):
            at = pl.ds(pl.multiple_of(i * bm, bm), bm)
            part[r, at, :] = lax.dot_general(
                hidden[at, :], down[where, :], (((1,), (1,)), ((), ())),
                preferred_element_type=jnp.float32).astype(jnp.bfloat16)

        @pl.when(r // per_owner % 2 != core)
        def _():
            pair_copy(r).start()

    def pair_sum(r):
        owner = r // per_owner

        @pl.when(owner % 2 == core)
        def _():
            pair_copy(r).wait_recv()

            @pl.loop(0, tokens // tile)
            def _(i):
                at = pl.ds(pl.multiple_of(i * tile, tile), tile)
                both = part[r, at, :].astype(jnp.float32) + pair[r, at, :].astype(jnp.float32)
                part[r, at, :] = both.astype(jnp.bfloat16)

            @pl.when(owner // 2 != group)
            def _():
                cross_copy(r, owner // 2, group).start()

    def at_distance(d, flip, fn):
        for sign in (-1, 1):
            at = z + sign * d

            @pl.when((at >= 0) & (at < chain))
            def _():
                fn(at * 2 + (y + flip) % 2)

    own_down.wait()
    multiply(fs)
    for k in mains:
        arrived(1, z * 2 + 1 - y, k)
    multiply(z * 2 + 1 - y)
    pair_sum(fs)
    at_distance(1, 0, multiply)
    pair_sum(z * 2 + 1 - y)

    @pl.loop(2, chain)
    def _(d):
        step_sends(1, d, lambda c: c.start(), True)
        side_arrivals(1, d - 1)
        at_distance(d - 1, 1, multiply)
        at_distance(d - 1, 0, pair_sum)
        at_distance(d, 0, multiply)
        at_distance(d - 1, 1, pair_sum)

    at_distance(chain - 1, 0, pair_sum)
    side_arrivals(1, chain - 1)
    at_distance(chain - 1, 1, multiply)
    at_distance(chain - 1, 1, pair_sum)

    for s in range(per_owner):
        r = me * per_owner + s
        for g in range(1, groups):
            other = lax.rem(group + g, groups)
            cross_copy(r, other, other).wait_recv()

        @pl.loop(0, tokens // tile)
        def _(i):
            at = pl.ds(pl.multiple_of(i * tile, tile), tile)
            value = part[r, at, :].astype(jnp.float32)
            for g in range(1, groups):
                value = value + cross[lax.rem(group + g, groups), s, at, :].astype(jnp.float32)
            total[at, s * rows:(s + 1) * rows] = value.astype(jnp.bfloat16)

    mixed_write = pltpu.make_async_copy(total, mixed_out, local_sem.at[0])
    mixed_write.start()

    for m in (0, 1):
        for way, k in own_sends(m):
            when_way(way, lambda way=way, k=k: copy(m, fs, k, way, True).wait_send())
        relay_own_extra(m, lambda c: c.wait_send())

        @pl.loop(1, chain)
        def _(d):
            step_sends(m, d, lambda c: c.wait_send(), False)

    @pl.loop(0, n)
    def _(r):
        owner = r // per_owner

        @pl.when(owner % 2 != core)
        def _():
            pair_copy(r).wait_send()

        @pl.when((owner % 2 == core) & (owner // 2 != group))
        def _():
            cross_copy(r, owner // 2, group).wait_send()

        block_write(r).wait()

    up_write.wait()
    mixed_write.wait()


def on_device(n, tp, tokens, norm_gain, up_weight, down_weight):
    up_local = (norm_gain[:, None] * up_weight).astype(jnp.bfloat16)
    down_local = down_weight.astype(jnp.bfloat16)
    rows, units = up_local.shape
    count, width = tokens.shape
    bf16 = jnp.bfloat16
    groups, per_owner = tp // 2, n // tp
    chunks = len(chunks_of(rows))
    features = width * tp
    dma = pltpu.SemaphoreType.DMA
    flops = 2 * 2 * count * features * units
    return tuple(pl.pallas_call(
        functools.partial(kernel, n, tp),
        out_shape=(jax.ShapeDtypeStruct((features, units), bf16), jax.ShapeDtypeStruct((features, units), bf16),
                   jax.ShapeDtypeStruct((count, width), bf16)),
        in_specs=[pl.BlockSpec(memory_space=pltpu.VMEM)] * 3,
        out_specs=[pl.BlockSpec(memory_space=pl.ANY)] * 3,
        scratch_shapes=[
            pltpu.VMEM((count, features), bf16),
            pltpu.VMEM((features, units), bf16),
            pltpu.VMEM((features, units), bf16),
            pltpu.VMEM((count, units), bf16),
            pltpu.VMEM((n, count, rows), bf16),
            pltpu.VMEM((n, count, rows), bf16),
            pltpu.VMEM((groups, per_owner, count, rows), bf16),
            pltpu.VMEM((count, width), bf16),
            dma((2, 3, n, chunks)), dma((2, n, chunks)),
            dma((2 * groups,)), dma((tp,)),
            dma((n,)), dma((n,)), dma((n,)), dma((groups, per_owner)),
            dma((3 + n,)),
        ],
        cost_estimate=pl.CostEstimate(flops=flops, bytes_accessed=4 * features * units * 2, transcendentals=0),
        compiler_params=pltpu.CompilerParams(
            collective_id=0, has_side_effects=True, vmem_limit_bytes=67043328),
    )(tokens, up_local, down_local))


def solution(mesh):
    return jax.shard_map(
        functools.partial(on_device, mesh.shape["fs"], mesh.shape["tp"]),
        mesh=mesh,
        in_specs=(P("fs", "tp"), P("fs"), P("fs", "tp"), P("fs", "tp")),
        out_specs=(P(None, "tp"), P(None, "tp"), P("fs", "tp")),
        check_vma=False,
    )
```

time: 426 us -> 225 us (0.53)
  waiting for transfers between devices: 348 us -> 0 us
  Pallas kernels: 0 us -> 202 us
  matrix products: 34.7 us -> 0 us
  between operations: 13.8 us -> 0.65 us
  other arithmetic: 9.54 us -> 4 us
    all_gather x3 -> x0, waiting for transfers between devices: 290 us -> none  [the longest x1 125 us: on_device(): block_rows = lax.all_gather(down_local, 'fs', axis=0, tiled=True)]
    pallas_call x0 -> x1, Pallas kernels: none -> 202 us  [on_device(): pl.pallas_call(functools.partial(kernel, n, tp), out_shape=(jax.ShapeDtyp...]
    reduce_scatter x1 -> x0, waiting for transfers between devices: 56.8 us -> none  [on_device(): lax.psum_scatter(rounded.astype(jnp.bfloat16), 'tp', scatter_dimension=1,...]
    dot_general x1 -> x0, matrix products: 34.7 us -> none  [on_device(): lax.dot_general(hidden, block_rows, (((1,), (1,)), ((), ())), preferred_e...]
    unnamed x2 -> x7, local copies, waits for them, and re-layouts: 16.9 us -> 18.2 us
  transfers between devices with their start and end apart: 4 -> 0, of which waited for: 4 -> 0; matrix products, arithmetic and copies ran while one was open for 2% -> 0% of each run, Pallas kernels for 0% -> 0%
where the time goes in v1:
time: 225 us; the launch traced here: 224 us
  Pallas kernels  202 us (90%)
  local copies, waits for them, and re-layouts  18.2 us (8%)
  other arithmetic  4 us (2%)
    pallas_call x1, Pallas kernels, on_device(): pl.pallas_call(functools.partial(kernel, n, tp), out_shape=(jax.ShapeDtyp...  202 us
    unnamed x7, local copies, waits for them, and re-layouts  18.2 us

profile of v1, /device:TPU:7, one launch (start us, length us, event | category | flops | bytes accessed | tf_op | source)
XLA Modules:
  0.0 224.4 jit_solution(9627671267794520498)
XLA Ops:
  0.6 0.0 copy-start
  0.6 2.9 %multiply_convert_fusion.upl = bf16[256,2048]{1,0:T(8,128)(2,1)} fusion(f32[256,2048]{1,0:T(8,128)} %param.6, f32[256]{0:T(256)} %param.5), kind=kLoop, calls=%fused_computation | loop fusion | flops 1048576 | bytes 3146752 | tf_op jit(solution)/shard_map/convert_element_type | solution.py:323
  3.5 0.0 copy-done
  3.5 1.1 convert_element_type.7.downl
  4.6 201.6 %shard_map.67 = (bf16[2048,2048]{1,0:T(8,128)(2,1)}, bf16[2048,2048]{1,0:T(8,128)(2,1)}, bf16[1536,512]{1,0:T(8,128)(2,1)}) custom-call(bf16[1536,512]{1,0:T(8,128)(2,1)} %tok_in.1, bf16[256,2048]{1,0:T(8,128)(2,1)} %multiply_convert_fusion.upl, bf16[256,2048]{1,0:T(8,128)(2,1)} %convert_element_type.7.downl), custom_call_target="tpu_custom_call" | custom-call | flops 25769803776 | bytes 33554432 | tf_op jit(solution)/shard_map/pallas_call | solution.py:333
  206.2 8.4 %copy.10 = bf16[2048,2048]{1,0:T(8,128)(2,1)} copy(bf16[2048,2048]{1,0:T(8,128)(2,1)} %get-tuple-element.6) | data formatting | bytes 16777216
  214.7 0.0 copy-start.1
  214.7 8.6 %copy.11 = bf16[2048,2048]{1,0:T(8,128)(2,1)} copy(bf16[2048,2048]{1,0:T(8,128)(2,1)} %get-tuple-element.7) | data formatting | bytes 16777216
  223.2 0.0 copy-done.1
  223.2 1.1 copy.12
Async XLA Ops:
  0.6 2.9 %copy-start = (f32[256,2048]{1,0:T(8,128)S(1)}, f32[256,2048]{1,0:T(8,128)}, u32[]{:S(2)}) copy-start(f32[256,2048]{1,0:T(8,128)} %param.7) | copy-start | bytes 6291460
  214.7 8.6 %copy-start.1 = (bf16[1536,512]{1,0:T(8,128)(2,1)S(1)}, bf16[1536,512]{1,0:T(8,128)(2,1)}, u32[]{:S(2)}) copy-start(bf16[1536,512]{1,0:T(8,128)(2,1)} %get-tuple-element.8) | copy-start | bytes 4718596

commit v2 on v1

v2 whole, which is shorter than its diff:
```python
import functools

import jax
import jax.numpy as jnp
from jax import lax
from jax.experimental import pallas as pl
from jax.experimental.pallas import tpu as pltpu
from jax.sharding import PartitionSpec as P

epsilon = 1e-06
MESH = pl.DeviceIdType.MESH
UP, DOWN, SIDE = 0, 1, 2


def chunks_of(rows, m):
    extra = max(16, rows * (2 + m) // 16 // 16 * 16)
    main, half = rows - extra, rows // 2
    if half % 128 == 0:
        return [(0, half), (half, main - half), (main, extra)]
    return [(0, main), (main, extra)]


def kernel(n, tp, tok_in, gain, up_weight, down_weight, up, down, total,
           stage, tok, hidden, part, pair, cross,
           send_sem, recv_sem, tok_send, tok_recv, pair_send, pair_recv, cross_send, cross_recv, local_sem):
    rows, units = up_weight.shape
    tokens, width = tok_in.shape
    chain = n // 2
    groups = tp // 2
    per_owner = n // tp
    chunks = [chunks_of(rows, 0), chunks_of(rows, 1)]
    extra = len(chunks[0]) - 1
    mains = range(extra)
    halves = extra
    half_rows = rows // halves
    fs, me = lax.axis_index("fs"), lax.axis_index("tp")
    z, y = fs // 2, fs % 2
    group, core = me // 2, me % 2
    partner = group * 2 + 1 - core
    bufs = (up, down)

    def target(way):
        if way == UP:
            return {"fs": jnp.minimum(z + 1, chain - 1) * 2 + y}
        if way == DOWN:
            return {"fs": jnp.maximum(z - 1, 0) * 2 + y}
        return {"fs": z * 2 + 1 - y}

    def spot(m, src, k):
        return pl.ds(pl.multiple_of(pl.multiple_of(src * rows, 16) + chunks[m][k][0], 16), chunks[m][k][1])

    def copy(m, src, k, way):
        where = spot(m, src, k)
        return pltpu.make_async_remote_copy(
            src_ref=bufs[m].at[where],
            dst_ref=bufs[m].at[where],
            send_sem=send_sem.at[m, way, src, k],
            recv_sem=recv_sem.at[m, src, k],
            device_id=target(way),
            device_id_type=MESH,
        )

    def arrived(m, src, k):
        where = spot(m, src, k)
        pltpu.make_async_remote_copy(
            src_ref=bufs[m].at[where], dst_ref=bufs[m].at[where],
            send_sem=send_sem.at[m, SIDE, src, k], recv_sem=recv_sem.at[m, src, k],
            device_id=target(SIDE), device_id_type=MESH,
        ).wait_recv()

    def own_sends(m):
        order = [(SIDE, extra)] + [(way, k) for k in mains for way in (UP, DOWN, SIDE)] + [(UP, extra), (DOWN, extra)]
        return [(way, k) for way, k in order]

    def when_way(way, fn):
        if way == UP:
            pl.when(z < chain - 1)(fn)
        elif way == DOWN:
            pl.when(z > 0)(fn)
        else:
            fn()

    def start_own(m):
        for way, k in own_sends(m):
            when_way(way, lambda way=way, k=k: copy(m, fs, k, way).start())

    def relay_own_extra(m, act):
        other = z * 2 + 1 - y
        for way in (UP, DOWN):
            when_way(way, lambda way=way: act(copy(m, other, extra, way)))

    def step_sends(m, d, act, wait):
        plan = [(k, 0) for k in mains] + [(extra, 0), (extra, 1)]
        for k, flip in plan:
            for sign, way in ((-1, UP), (1, DOWN)):
                at = z + sign * d
                src = at * 2 + (y + flip) % 2

                @pl.when((at >= 0) & (at < chain))
                def _():
                    if wait:
                        arrived(m, src, k)
                    when_way(way, lambda: act(copy(m, src, k, way)))
                    if k != extra:
                        act(copy(m, src, k, SIDE))

    def side_arrivals(m, d):
        for sign in (-1, 1) if not (isinstance(d, int) and d == 0) else (1,):
            at = z + sign * d

            @pl.when((at >= 0) & (at < chain))
            def _():
                for k in mains:
                    arrived(m, at * 2 + 1 - y, k)

    own_rows = pl.ds(pl.multiple_of(fs * rows, 16), rows)
    loads = [pltpu.make_async_copy(up_weight, stage.at[0], local_sem.at[1]),
             pltpu.make_async_copy(tok_in, tok.at[:, pl.ds(pl.multiple_of(me * width, 128), width)], local_sem.at[0]),
             pltpu.make_async_copy(down_weight, stage.at[1], local_sem.at[2])]
    for load in loads:
        load.start()

    barrier = pltpu.get_barrier_semaphore()
    greet = [{"fs": lax.rem(z + 1, chain) * 2 + y}, {"fs": lax.rem(z + chain - 1, chain) * 2 + y},
             {"fs": z * 2 + 1 - y}, {"tp": partner}]
    greet += [{"tp": lax.rem(group + g, groups) * 2 + core} for g in range(1, groups)]
    for who in greet:
        pl.semaphore_signal(barrier, inc=1, device_id=who, device_id_type=MESH)
    loads[0].wait()
    by_row = jnp.transpose(jnp.broadcast_to(gain[...], (128, rows)))[:, :1]
    up[own_rows, :] = (by_row * stage[0]).astype(jnp.bfloat16)
    pl.semaphore_wait(barrier, len(greet))

    start_own(0)
    loads[1].wait()

    def columns(owner):
        return pl.ds(pl.multiple_of(owner * width, 128), width)

    def token_copy(owner, to, slot):
        return pltpu.make_async_remote_copy(
            src_ref=tok.at[:, columns(owner)],
            dst_ref=tok.at[:, columns(owner)],
            send_sem=tok_send.at[slot], recv_sem=tok_recv.at[owner],
            device_id={"tp": to}, device_id_type=MESH)

    across = [lax.rem(group + g, groups) * 2 + core for g in range(1, groups)]
    back = [lax.rem(group + groups - g, groups) * 2 + core for g in range(1, groups)]
    token_sends = [token_copy(me, to, i) for i, to in enumerate(across)]
    token_sends.append(token_copy(me, partner, groups - 1))
    for c in token_sends:
        c.start()
    loads[2].wait()
    down[own_rows, :] = stage[1].astype(jnp.bfloat16)

    arrived(0, z * 2 + 1 - y, extra)
    relay_own_extra(0, lambda c: c.start())
    step_sends(0, 1, lambda c: c.start(), True)

    relays = []
    for i, owner in enumerate(back):
        token_copy(owner, partner, groups + i).wait_recv()
        c = token_copy(owner, partner, groups + i)
        c.start()
        relays.append(c)
    token_copy(partner, partner, 0).wait_recv()
    for g in range(1, groups):
        token_copy(lax.rem(group + g, groups) * 2 + 1 - core, partner, 0).wait_recv()
    for c in token_sends + relays:
        c.wait_send()
    tile = 128

    @pl.loop(0, tokens // tile)
    def _(i):
        at = pl.ds(pl.multiple_of(i * tile, tile), tile)
        wide = tok[at, :].astype(jnp.float32)
        scale = lax.rsqrt(jnp.mean(wide * wide, axis=-1, keepdims=True) + epsilon)
        tok[at, :] = (wide * scale).astype(jnp.bfloat16)

    for d in range(2, chain):
        step_sends(0, d, lambda c: c.start(), True)
    start_own(1)
    for d in range(chain):
        side_arrivals(0, d)
    bm, bn = min(512, tokens), min(512, units)

    def expand(first, last):
        @pl.loop(first, last)
        def _(j):
            cols = pl.ds(pl.multiple_of(j * bn, bn), bn)

            @pl.loop(0, tokens // bm)
            def _(i):
                at = pl.ds(pl.multiple_of(i * bm, bm), bm)
                values = jnp.dot(tok[at, :], up[:, cols], preferred_element_type=jnp.float32)
                values = jnp.maximum(values, 0.0)
                hidden[at, cols] = (values * values).astype(jnp.bfloat16)

    expand(0, units // bn // 2)
    arrived(1, z * 2 + 1 - y, extra)
    relay_own_extra(1, lambda c: c.start())
    step_sends(1, 1, lambda c: c.start(), True)
    expand(units // bn // 2, units // bn)

    def pair_copy(r, h):
        return pltpu.make_async_remote_copy(
            src_ref=part.at[r, h], dst_ref=pair.at[r, h], send_sem=pair_send.at[r, h], recv_sem=pair_recv.at[r, h],
            device_id={"tp": partner}, device_id_type=MESH)

    def cross_copy(r, h, to_group, from_group):
        slot = r % per_owner
        return pltpu.make_async_remote_copy(
            src_ref=part.at[r, h], dst_ref=cross.at[from_group, slot, h],
            send_sem=cross_send.at[r, h], recv_sem=cross_recv.at[from_group, slot, h],
            device_id={"tp": to_group * 2 + core}, device_id_type=MESH)

    def multiply(r, hs):
        where = pl.ds(pl.multiple_of(r * rows + hs[0] * half_rows, 16), len(hs) * half_rows)

        @pl.loop(0, tokens // bm)
        def _(i):
            at = pl.ds(pl.multiple_of(i * bm, bm), bm)
            values = lax.dot_general(
                hidden[at, :], down[where, :], (((1,), (1,)), ((), ())),
                preferred_element_type=jnp.float32).astype(jnp.bfloat16)
            for i_h, h in enumerate(hs):
                part[r, h, at, :] = values[:, i_h * half_rows:(i_h + 1) * half_rows]

        @pl.when(r // per_owner % 2 != core)
        def _():
            for h in hs:
                pair_copy(r, h).start()

    def pair_sum(r, hs):
        owner = r // per_owner

        @pl.when(owner % 2 == core)
        def _():
            for h in hs:
                pair_copy(r, h).wait_recv()

                @pl.loop(0, tokens // tile)
                def _(i):
                    at = pl.ds(pl.multiple_of(i * tile, tile), tile)
                    both = part[r, h, at, :].astype(jnp.float32) + pair[r, h, at, :].astype(jnp.float32)
                    part[r, h, at, :] = both.astype(jnp.bfloat16)

                @pl.when(owner // 2 != group)
                def _():
                    cross_copy(r, h, owner // 2, group).start()

    def at_distance(d, flip, fn):
        for sign in (-1, 1):
            at = z + sign * d

            @pl.when((at >= 0) & (at < chain))
            def _():
                fn(at * 2 + (y + flip) % 2)

    every = list(range(halves))

    def side_block(r):
        for h in every:
            arrived(1, r, h)
            multiply(r, [h])
            pair_sum(r, [h])

    multiply(fs, every)
    side_block(z * 2 + 1 - y)
    pair_sum(fs, every)
    at_distance(1, 0, lambda r: multiply(r, every))

    @pl.loop(2, chain)
    def _(d):
        step_sends(1, d, lambda c: c.start(), True)
        at_distance(d - 1, 0, lambda r: pair_sum(r, every))
        at_distance(d - 1, 1, side_block)
        at_distance(d, 0, lambda r: multiply(r, every))

    at_distance(chain - 1, 0, lambda r: pair_sum(r, every))
    at_distance(chain - 1, 1, side_block)

    for s in range(per_owner):
        r = me * per_owner + s
        for h in every:
            for g in range(1, groups):
                other = lax.rem(group + g, groups)
                cross_copy(r, h, other, other).wait_recv()

            @pl.loop(0, tokens // tile)
            def _(i):
                at = pl.ds(pl.multiple_of(i * tile, tile), tile)
                value = part[r, h, at, :].astype(jnp.float32)
                for g in range(1, groups):
                    value = value + cross[lax.rem(group + g, groups), s, h, at, :].astype(jnp.float32)
                first = s * rows + h * half_rows
                total[at, first:first + half_rows] = value.astype(jnp.bfloat16)

    for m in (0, 1):
        for way, k in own_sends(m):
            when_way(way, lambda way=way, k=k: copy(m, fs, k, way).wait_send())
        relay_own_extra(m, lambda c: c.wait_send())

        @pl.loop(1, chain)
        def _(d):
            step_sends(m, d, lambda c: c.wait_send(), False)

    @pl.loop(0, n)
    def _(r):
        owner = r // per_owner

        @pl.when(owner % 2 != core)
        def _():
            for h in every:
                pair_copy(r, h).wait_send()

        @pl.when((owner % 2 == core) & (owner // 2 != group))
        def _():
            for h in every:
                cross_copy(r, h, owner // 2, group).wait_send()


def on_device(n, tp, tokens, norm_gain, up_weight, down_weight):
    rows, units = up_weight.shape
    count, width = tokens.shape
    bf16 = jnp.bfloat16
    groups, per_owner = tp // 2, n // tp
    chunks = len(chunks_of(rows, 0))
    halves = chunks - 1
    half_rows = rows // halves
    features = width * tp
    dma = pltpu.SemaphoreType.DMA
    flops = 2 * 2 * count * features * units
    return tuple(pl.pallas_call(
        functools.partial(kernel, n, tp),
        out_shape=(pltpu.VMEM((features, units), bf16), pltpu.VMEM((features, units), bf16),
                   pltpu.VMEM((count, width), bf16)),
        in_specs=[pl.BlockSpec(memory_space=pl.ANY if i != 1 else pltpu.VMEM) for i in range(4)],
        out_specs=[pl.BlockSpec(memory_space=pltpu.VMEM)] * 3,
        scratch_shapes=[
            pltpu.VMEM((2, rows, units), jnp.float32),
            pltpu.VMEM((count, features), bf16),
            pltpu.VMEM((count, units), bf16),
            pltpu.VMEM((n, halves, count, half_rows), bf16),
            pltpu.VMEM((n, halves, count, half_rows), bf16),
            pltpu.VMEM((groups, per_owner, halves, count, half_rows), bf16),
            dma((2, 3, n, chunks)), dma((2, n, chunks)),
            dma((2 * groups,)), dma((tp,)),
            dma((n, halves)), dma((n, halves)), dma((n, halves)), dma((groups, per_owner, halves)),
            dma((3,)),
        ],
        cost_estimate=pl.CostEstimate(flops=flops, bytes_accessed=4 * features * units * 2, transcendentals=0),
        compiler_params=pltpu.CompilerParams(
            collective_id=0, has_side_effects=True, vmem_limit_bytes=44 << 20),
    )(tokens, norm_gain[None, :], up_weight, down_weight))


def solution(mesh):
    return jax.shard_map(
        functools.partial(on_device, mesh.shape["fs"], mesh.shape["tp"]),
        mesh=mesh,
        in_specs=(P("fs", "tp"), P("fs"), P("fs", "tp"), P("fs", "tp")),
        out_specs=(P(None, "tp"), P(None, "tp"), P("fs", "tp")),
        check_vma=False,
    )
```

time: 225 us -> 209 us (0.929)
  local copies, waits for them, and re-layouts: 18.2 us -> 7.94 us
  other arithmetic: 4 us -> 0 us
    unnamed x7 -> x3, local copies, waits for them, and re-layouts: 18.2 us -> 7.94 us
    convert_element_type x2 -> x0, other arithmetic: 4 us -> none  [the longest x1 2.89 us: on_device(): up_local = (norm_gain[:, None] * up_weight).astype(jnp.bfloat16)]
where the time goes in v2:
time: 209 us
  Pallas kernels  200 us (96%)
  local copies, waits for them, and re-layouts  7.94 us (4%)
    pallas_call x1, Pallas kernels, on_device(): pl.pallas_call(functools.partial(kernel, n, tp), out_shape=(pltpu.VMEM((f...  200 us
    unnamed x3, local copies, waits for them, and re-layouts  7.94 us

profile of v2, /device:TPU:7, one launch (start us, length us, event | category | flops | bytes accessed | tf_op | source)
XLA Modules:
  0.0 208.5 jit_solution(3740334233674571696)
XLA Ops:
  0.6 199.9 %shard_map.67 = (bf16[2048,2048]{1,0:T(8,128)(2,1)S(1)}, bf16[2048,2048]{1,0:T(8,128)(2,1)S(1)}, bf16[1536,512]{1,0:T(8,128)(2,1)S(1)}) custom-call(bf16[1536,512]{1,0:T(8,128)(2,1)} %tok_in.1, f32[1,256]{1,0:T(1,128)} %bitcast.1, f32[256,2048]{1,0:T(8,128)} %up_weight.1, f32[256,2048]{1,0:T(8,128)} %down_weight.1), custom_call_target="tpu_custom_call" | custom-call | flops 25769803776 | bytes 33554432 | tf_op jit(solution)/shard_map/pallas_call | solution.py:334
  200.6 3.4 %copy.10 = bf16[2048,2048]{1,0:T(8,128)(2,1)} copy(bf16[2048,2048]{1,0:T(8,128)(2,1)S(1)} %get-tuple-element.3) | data formatting | bytes 16777216
  204.0 1.1 copy.12
  205.1 3.4 %copy.11 = bf16[2048,2048]{1,0:T(8,128)(2,1)} copy(bf16[2048,2048]{1,0:T(8,128)(2,1)S(1)} %get-tuple-element.4) | data formatting | bytes 16777216
